TPU v7x, 512 devices: a whole 4x4x16 slice. The times are simulated.
512 devices in a mesh: sp: 64 (over z, y), tp: 8 (over x, core).
Axes of the slice: x: 4, y: 4, z: 16, core: 2. Of those that a mesh axis runs over, the one named last changes fastest.
Arguments:
- residual: bfloat16 [16384, 2048], P('sp'), may hold values from -6 to 6
- queries: bfloat16 [16384, 1024], P('sp', 'tp'), may hold values from -6 to 6
- forget_gate_logits: bfloat16 [16384, 1024], P('sp', 'tp'), may hold values from -5 to 5
- projected_values: bfloat16 [16384, 1024], P('sp', 'tp'), may hold values from -6 to 6
- output_gate_logits: bfloat16 [16384, 1024], P('sp', 'tp'), may hold values from -6 to 6
- lower_bound_margin: float32 [1024], P('tp'), may hold values from 6.1035156e-05 to 0.08
- extra_forget_logs: float32 [16384, 1024], P('sp', 'tp'), may hold values from -0.7 to 0
- per_head_norm_gain: float32 [128], replicated, may hold values from 0.1 to 1.9
- output_weight: bfloat16 [1024, 2048], P('tp'), may hold values from -0.1875 to 0.1875
- feedforward_norm_gain: float32 [2048], replicated, may hold values from 0.1 to 1.9
- gate_weight: bfloat16 [2048, 5632], P('sp', 'tp'), may hold values from -0.125 to 0.125
- up_weight: bfloat16 [2048, 5632], P('sp', 'tp'), may hold values from -0.125 to 0.125
- down_weight: bfloat16 [5632, 2048], P('tp', 'sp'), may hold values from -0.078125 to 0.078125
Outputs:
- layer_out: bfloat16 [16384, 2048], P('sp')
All inputs are finite; a program needn't handle non-finite values.
Results may differ from a plain program's by a relative error of at most 0.015.
Values may be sent and summed in bfloat16 or wider, within the bound.
No kernel may reach another device: no remote copies, remote signals or barrier semaphores. Data moves between devices by JAX's collectives and lax.ppermute only.
A program may use at most 64 MiB of HBM per device.

v0:
```python
import jax
import jax.numpy as jnp
from jax import lax
from jax.sharding import Mesh
from jax.sharding import PartitionSpec as P

HD = 128
BLOCK = 64
SP = ("sp_0", "sp_1")
eps = 1e-06


def gather_turned(arrays, axis, dims):
    turned = [jnp.moveaxis(a, dim, 0) for a, dim in zip(arrays, dims)]
    widths = [t[0].size for t in turned]
    both = jnp.concatenate([t.reshape(-1, w) for t, w in zip(turned, widths)], axis=1)
    filled = lax.all_gather(both, axis, axis=0, tiled=True)
    parts = jnp.split(filled, [sum(widths[:k]) for k in range(1, len(widths))], axis=1)
    return tuple(
        (
            jnp.moveaxis(b.reshape(-1, *t.shape[1:]), 0, dim)
            for b, t, dim in zip(parts, turned, dims)
        )
    )


def nothing_yet(value, identity):
    return jax.tree.map(
        lambda a, e: jnp.broadcast_to(jnp.asarray(e, a.dtype), a.shape), value, identity
    )


def gathered_once(value, axis):
    leaves = jax.tree.leaves(value)
    order = sorted(range(len(leaves)), key=lambda k: -leaves[k].size)
    width = (1, *leaves[order[0]].shape)[-1]
    lines = [
        jnp.pad(leaves[k].reshape(-1), (0, -leaves[k].size % width)).reshape(-1, width)
        for k in order
    ]
    both, at, found = (lax.all_gather(jnp.concatenate(lines), axis), 0, {})
    for k, line in zip(order, lines):
        section = both[:, at : at + len(line)].reshape(len(both), -1)
        found[k] = section[:, : leaves[k].size].reshape(-1, *leaves[k].shape)
        at += len(line)
    numbers = iter(range(len(leaves)))
    return jax.tree.map(lambda _: found[next(numbers)], value)


def carried_in_2(value, axes, combine, identity):
    before = start = nothing_yet(value, identity)
    running = value
    for axis in reversed(axes):
        length, place = (lax.axis_size(axis), lax.axis_index(axis))
        pieces = gathered_once(
            jax.tree.map(
                lambda part, kind: part.astype(kind), running, (jnp.bfloat16, jnp.bfloat16)
            ),
            axis,
        )
        inside, running = (start, start)
        for k in range(length):
            passed = k < place
            running = combine(
                running, jax.tree.map(lambda part, own: part[k].astype(own.dtype), pieces, value)
            )
            inside = jax.tree.map(lambda new, old: jnp.where(passed, new, old), running, inside)
        before = combine(inside, before)
    return before


def cut_along(value, dim, length):
    shape = value.shape
    parts = value.reshape(*shape[:dim], length, shape[dim] // length, *shape[dim + 1 :])
    return jnp.moveaxis(parts, dim, 0)


def sum_at_owner(value, axis, dim):
    parts = cut_along(value, dim, lax.axis_size(axis))
    arrived = lax.all_to_all(parts, axis, split_axis=0, concat_axis=0, tiled=True)
    return arrived.astype(jnp.float32).sum(axis=0)


def copy_for_each(value, axis):
    copies = jnp.broadcast_to(value, (lax.axis_size(axis), *value.shape))
    return lax.all_to_all(copies, axis, split_axis=0, concat_axis=0, tiled=True)


def laid_out(parts, dim):
    shape = list(parts.shape[1:])
    shape[dim] *= parts.shape[0]
    return jnp.moveaxis(parts, 0, dim).reshape(shape)


def collect(value, axis, dim):
    parts = copy_for_each(value, axis)
    return laid_out(parts, dim)


def block_update(carried_in, inputs):
    recurrent_state, offset = carried_in
    queries, state_increment, value_rows, retain_log_factor = inputs
    running_state = jnp.cumsum(retain_log_factor, axis=1)
    causal = jnp.tril(
        jnp.ones((retain_log_factor.shape[1], retain_log_factor.shape[1]), dtype=bool)
    )
    carried_over_state = jnp.einsum(
        "uqw,uwa->uqa", queries * jnp.exp(running_state), recurrent_state
    )
    spread = running_state[:, :, None, :] - running_state[:, None, :, :]
    weights = jnp.exp(jnp.where(causal[None, :, :, None], spread, -jnp.inf))
    scores = jnp.einsum("htk,htsk,hsk->hts", queries, weights, state_increment)
    output_rows = carried_over_state + jnp.einsum("hts,hsv->htv", scores, value_rows)
    final_state = running_state[:, -1:, :]
    updated_state = jnp.exp(final_state[:, 0, :])[:, :, None] * recurrent_state + jnp.einsum(
        "erb,erc->ebc", state_increment * jnp.exp(final_state - running_state), value_rows
    )
    rescaled_state = queries * jnp.exp(running_state + offset[:, None, :])
    return ((updated_state, offset + final_state[:, 0, :]), (output_rows, rescaled_state))


def join_states(earlier, later):
    earlier_sum, earlier_memory = earlier
    later_sum, later_memory = later
    return (earlier_sum + later_sum, jnp.exp(later_sum)[:, :, None] * earlier_memory + later_memory)


def local(
    residual,
    queries,
    forget_gate_logits,
    projected_values,
    output_gate_logits,
    lower_bound_margin,
    extra_forget_logs,
    per_head_norm_gain,
    output_weight,
    feedforward_norm_gain,
    gate_weight,
    up_weight,
    down_weight,
):
    gate_full, up_full, down_full = gather_turned(
        (gate_weight, up_weight, down_weight), SP, (0, 0, 1)
    )
    length = queries.shape[0]
    head_count = queries.shape[1] // HD
    state_increment = lower_bound_margin * jax.nn.sigmoid(-forget_gate_logits.astype(jnp.float32))
    retain_log_factor = jnp.log1p(-state_increment) + extra_forget_logs

    def to_blocks(source):
        return source.reshape(length // BLOCK, BLOCK, head_count, HD).transpose(0, 2, 1, 3)

    initial = (
        jnp.zeros((head_count, HD, HD), jnp.float32),
        jnp.zeros((head_count, HD), jnp.float32),
    )
    block_inputs = (
        to_blocks(queries.astype(jnp.float32)),
        to_blocks(state_increment),
        to_blocks(projected_values.astype(jnp.float32)),
        to_blocks(retain_log_factor),
    )
    (recurrent_state, decay_sum), (output_rows, rescaled_state) = lax.scan(
        block_update, initial, block_inputs
    )
    identity = (jnp.zeros_like(decay_sum), jnp.zeros_like(recurrent_state))
    incoming_state = carried_in_2((decay_sum, recurrent_state), SP, join_states, identity)[1]
    output_rows = output_rows + jnp.einsum("sjey,jyx->sjex", rescaled_state, incoming_state)
    mixed = output_rows.transpose(0, 2, 1, 3).reshape(length, head_count, HD)
    normed_heads = (
        mixed
        * lax.rsqrt(jnp.mean(mixed * mixed, axis=-1, keepdims=True) + eps)
        * per_head_norm_gain
    )
    gating = jax.nn.silu(output_gate_logits.astype(jnp.float32)).reshape(length, head_count, HD)
    gated = (normed_heads * gating).reshape(length, head_count * HD).astype(jnp.bfloat16)
    row_count = residual.shape[0] // lax.axis_size("tp")
    own_rows = lax.dynamic_slice_in_dim(residual, lax.axis_index("tp") * row_count, row_count, 0)
    rows_here = gated
    projected = sum_at_owner(
        jnp.dot(rows_here, output_weight, preferred_element_type=jnp.float32).astype(jnp.bfloat16),
        "tp",
        0,
    )
    after_mixer = (own_rows.astype(jnp.float32) + projected).astype(jnp.bfloat16)
    widened = after_mixer.astype(jnp.float32)
    normed = (
        widened
        * lax.rsqrt(jnp.mean(widened * widened, axis=-1, keepdims=True) + eps)
        * feedforward_norm_gain
    ).astype(jnp.bfloat16)
    row_piece = collect(normed, "tp", 0)
    gate_part = jnp.dot(row_piece, gate_full, preferred_element_type=jnp.float32)
    up_part = jnp.dot(row_piece, up_full, preferred_element_type=jnp.float32)
    hidden = (jax.nn.silu(gate_part) * up_part).astype(jnp.bfloat16)
    rows_here = hidden
    ffn_sum = sum_at_owner(
        jnp.dot(rows_here, down_full, preferred_element_type=jnp.float32).astype(jnp.bfloat16),
        "tp",
        0,
    )
    finished = (after_mixer.astype(jnp.float32) + 0.5 * ffn_sum).astype(jnp.bfloat16)
    return collect(finished, "tp", 0)


def solution(mesh):
    finer = Mesh(mesh.devices.reshape(16, 4, mesh.shape["tp"]), ("sp_0", "sp_1", "tp"))
    placed = (
        P(SP, None),
        P(SP, "tp"),
        P(SP, "tp"),
        P(SP, "tp"),
        P(SP, "tp"),
        P("tp"),
        P(SP, "tp"),
        P(),
        P("tp", None),
        P(),
        P(SP, "tp"),
        P(SP, "tp"),
        P("tp", SP),
    )
    return jax.shard_map(local, mesh=finer, in_specs=placed, out_specs=P(SP, None), check_vma=False)
```

profile of v0, /device:TPU:1, one launch (start us, length us, event | category | flops | bytes accessed | tf_op | source)
XLA Modules:
  0.0 229.9 jit_solution(110097667597470803)
XLA Ops:
  6.5 1.7 concatenate.11
  8.3 0.9 convert.7
  9.2 1.1 divide_multiply_fusion
  10.2 6.6 %while.17 = (s32[]{:T(128)}, f32[1,128,128]{2,1,0:T(8,128)S(1)}, f32[1,128]{1,0:T(1,128)S(1)}, f32[4,1,64,128]{3,2,1,0:T(8,128)S(1)}, bf16[4,1,64,128]{3,2,1,0:T...) while((s32[]{:T(128)}, f32[1,128,128]{2,1,0:T(8,128)S(1)}, ...), condition=%wide.region_2.3_spmd.clone, body=%wide.region_0.2_spmd.clone.sunk | while | flops 8499459 | bytes 1212596 | solution.py:164
  10.5 0.9 fusion.282
  11.4 0.1 fusion.281
  11.6 0.2 fusion.278
  12.1 0.9 fusion.282
  13.1 0.1 fusion.281
  13.2 0.2 fusion.278
  13.8 0.9 fusion.282
  14.7 0.1 fusion.281
  14.8 0.2 fusion.278
  15.4 0.9 fusion.282
  16.4 0.1 fusion.281
  16.5 0.2 fusion.278
  16.9 10.5 %all-gather.2 = bf16[4,129,128]{2,1,0:T(8,128)(2,1)S(1)} all-gather(bf16[1,129,128]{2,1,0:T(8,128)(2,1)S(1)} %maximum_bitcast_fusion), channel_id=2, replica_groups=mesh['sp_0'=16,'sp_1'=4,'tp'=8] {'sp_1'}, dimensions={0}, use_global_device_ids=true | all-gather | bytes 165120 | tf_op jit(solution)/shard_map/all_gather | solution.py:41
  27.5 33.0 %all-gather.3 = bf16[16,129,128]{2,1,0:T(8,128)(2,1)S(1)} all-gather(bf16[1,129,128]{2,1,0:T(8,128)(2,1)S(1)} %maximum_bitcast_fusion.1), channel_id=3, replica_groups=mesh['sp_0'=16,'sp_1'=4,'tp'=8] {'sp_0'}, dimensions={0}, use_global_device_ids=true | all-gather | bytes 561408 | tf_op jit(solution)/shard_map/all_gather | solution.py:41
  60.6 0.7 multiply_reduce_fusion
  61.5 1.4 convolution_convert_fusion
  62.9 14.1 %all-to-all-start = ((bf16[8,32,2048]{2,1,0:T(8,128)(2,1)}), bf16[8,32,2048]{2,1,0:T(8,128)(2,1)S(1)}, u32[]{:S(2)}, u32[]{:S(2)}) async-start(bf16[8,32,2048]{2,1,0:T(8,128)(2,1)} %bitcast.37), calls=%async_computation | async-start | bytes 2097152 | tf_op jit(solution)/shard_map/all_to_all | solution.py:80
  77.1 15.0 %all-to-all-done = bf16[8,32,2048]{2,1,0:T(8,128)(2,1)S(1)} async-done(((bf16[8,32,2048]{2,1,0:T(8,128)(2,1)}), bf16[8,32,2048]{2,1,0:T(8,128)(2,1)S(1)}, u32[]{:S(2)}, u32[]{:S(2)}) %all-to-all-start) | async-done | bytes 1048608 | tf_op jit(solution)/shard_map/all_to_all | solution.py:80
  92.0 0.1 convert_reduce_fusion.1
  92.2 1.1 fusion.65
  93.5 18.4 %all_to_all.20 = bf16[8,32,2048]{2,1,0:T(8,128)(2,1)S(1)} all-to-all(bf16[8,32,2048]{2,1,0:T(8,128)(2,1)S(1)} %broadcast_in_dim.28), channel_id=1, replica_groups=mesh['sp_0'=16,'sp_1'=4,'tp'=8] {'tp'}, dimensions={0} | all-to-all | bytes 2097152 | tf_op jit(solution)/shard_map/all_to_all | solution.py:86
  111.9 53.7 %all-gather.6.cloned.1.call-done = bf16[2048,2112]{1,0:T(8,128)(2,1)} async-done(((bf16[32,2112]{1,0:T(8,128)(2,1)}), bf16[2048,2112]{1,0:T(8,128)(2,1)}) %all-gather.6.cloned.1.call-update) | async-done | bytes 8650768 | tf_op jit(solution)/shard_map/all_gather | solution.py:17
  165.5 3.2 %fusion.45 = f32[256,704]{0,1:T(8,128)S(1)} fusion(bf16[256,2048]{1,0:T(8,128)(2,1)S(1)} %bitcast.209, bf16[2048,2112]{1,0:T(8,128)(2,1)} %all-gather.6.cloned.1.call-done), kind=kOutput, calls=%fused_computation.55 | convolution fusion | flops 738197504 | bytes 4915200 | tf_op jit(solution)/shard_map/dot_general | solution.py:194
  168.8 7.4 %fusion.47 = bf16[256,2048]{1,0:T(8,128)(2,1)S(1)} fusion(bf16[2048,2112]{1,0:T(8,128)(2,1)} %all-gather.6.cloned.1.call-done, bf16[256,2048]{1,0:T(8,128)(2,1)S(1)} %bitcast.210, f32[256,704]{0,1:T(8,128)S(1)} %fusion.45), kind=kOutput, calls=%fused_computation.58 | convolution fusion | flops 1478000640 | bytes 9109504 | tf_op jit(solution)/shard_map/dot_general | solution.py:199
  176.1 27.3 %all_to_all.21 = bf16[8,32,2048]{2,1,0:T(8,128)(2,1)S(1)} all-to-all(bf16[8,32,2048]{2,1,0:T(8,128)(2,1)S(1)} %bitcast.211), channel_id=1, replica_groups=mesh['sp_0'=16,'sp_1'=4,'tp'=8] {'tp'}, dimensions={0} | all-to-all | bytes 2097152 | tf_op jit(solution)/shard_map/all_to_all | solution.py:80
  203.4 0.1 convert_reduce_fusion
  203.7 18.4 %all_to_all.22 = bf16[8,32,2048]{2,1,0:T(8,128)(2,1)S(1)} all-to-all(bf16[8,32,2048]{2,1,0:T(8,128)(2,1)S(1)} %broadcast_in_dim.29), channel_id=1, replica_groups=mesh['sp_0'=16,'sp_1'=4,'tp'=8] {'tp'}, dimensions={0} | all-to-all | bytes 2097152 | tf_op jit(solution)/shard_map/all_to_all | solution.py:86
  222.1 1.0 copy.36
  (73 shorter events, 2.1 us)
Async XLA Ops:
  6.5 55.0 %copy-start = (bf16[128,2048]{1,0:T(8,128)(2,1)S(1)}, bf16[128,2048]{1,0:T(8,128)(2,1)}, u32[]{:S(2)}) copy-start(bf16[128,2048]{1,0:T(8,128)(2,1)} %param.23) | copy-start | bytes 1572868
  6.5 159.0 %all-gather.6.cloned.1.call-start = ((), (), s32[]{:S(2)}) async-start(), calls=%async_computation.4 | async-start | bytes 9052160 | tf_op jit(solution)/shard_map/all_gather | solution.py:17
  10.2 1.3 copy-start.1
  11.9 1.3 copy-start.1
  13.5 1.3 copy-start.1
  15.2 1.3 copy-start.1
  16.8 44.6 %copy-start.2 = (bf16[256,128]{1,0:T(8,128)(2,1)S(1)}, bf16[256,128]{1,0:T(8,128)(2,1)}, u32[]{:S(2)}) copy-start(bf16[256,128]{1,0:T(8,128)(2,1)} %param.19) | copy-start | bytes 196612
  16.8 44.6 %copy-start.4 = (f32[128]{0:T(128)S(1)}, f32[128]{0:T(128)}, u32[]{:S(2)}) copy-start(f32[128]{0:T(128)} %param.22) | copy-start | bytes 1540
  61.3 31.9 %copy-start.3 = (f32[2048]{0:T(1024)S(1)}, f32[2048]{0:T(1024)}, u32[]{:S(2)}) copy-start(f32[2048]{0:T(1024)} %param.24) | copy-start | bytes 24580
  62.9 29.1 %all-to-all-start = ((bf16[8,32,2048]{2,1,0:T(8,128)(2,1)}), bf16[8,32,2048]{2,1,0:T(8,128)(2,1)S(1)}, u32[]{:S(2)}, u32[]{:S(2)}) async-start(bf16[8,32,2048]{2,1,0:T(8,128)(2,1)} %bitcast.37), calls=%async_computation | async-start | bytes 2097152 | tf_op jit(solution)/shard_map/all_to_all | solution.py:80
Sparse Core Ops, SparseCore 0:
  10.3 155.2 all-gather.5
where the time goes:
time: 230 us
  blocking collectives  108 us (47%)
  waiting for transfers between devices  68.6 us (30%)
  matrix products  18.4 us (8%)
  starting transfers between devices  14.1 us (6%)
  between operations  13.6 us (6%)
  other arithmetic  4.28 us (2%)
  local copies, waits for them, and re-layouts  3.11 us (1%)
    all_gather x1, waiting for transfers between devices, gather_turned(): filled = lax.all_gather(both, axis, axis=0, tiled=True)  53.7 us
    all_gather x2, blocking collectives, gathered_once(): both, at, found = (lax.all_gather(jnp.concatenate(lines), axis), 0, {})  43.5 us
    all_to_all x2, blocking collectives, copy_for_each(): return lax.all_to_all(copies, axis, split_axis=0, concat_axis=0, tiled=True)  36.8 us
    all_to_all x1, blocking collectives, sum_at_owner(): lax.all_to_all(parts, axis, split_axis=0, concat_axis=0, tiled=True)  27.3 us
    all_to_all x1, waiting for transfers between devices, sum_at_owner(): lax.all_to_all(parts, axis, split_axis=0, concat_axis=0, tiled=True)  15 us
    all_to_all x1, starting transfers between devices, sum_at_owner(): lax.all_to_all(parts, axis, split_axis=0, concat_axis=0, tiled=True)  14.1 us
    dot_general x1, matrix products, local(): jnp.dot(rows_here, down_full, preferred_element_type=jnp.float32)  7.35 us
  transfers between devices with their start and end apart: 2, of which 2 were waited for; matrix products, arithmetic and copies ran while one was open for 5% of the time, Pallas kernels for 0%

commit v1 on v0

--- a/solution.py
+++ b/solution.py
@@ -14,7 +14,10 @@
     turned = [jnp.moveaxis(a, dim, 0) for a, dim in zip(arrays, dims)]
     widths = [t[0].size for t in turned]
     both = jnp.concatenate([t.reshape(-1, w) for t, w in zip(turned, widths)], axis=1)
-    filled = lax.all_gather(both, axis, axis=0, tiled=True)
+    count = lax.axis_size(axis)
+    shards = jnp.stack([both for _ in range(count)])
+    shards = lax.all_to_all(shards, axis, split_axis=0, concat_axis=0)
+    filled = jnp.concatenate(shards, axis=0)
     parts = jnp.split(filled, [sum(widths[:k]) for k in range(1, len(widths))], axis=1)
     return tuple(
         (

time: 230 us -> 564 us (2.45)
  blocking collectives: 108 us -> 480 us
  waiting for transfers between devices: 68.6 us -> 29.8 us
  between operations: 13.6 us -> 0.23 us
    all_to_all x0 -> x1, blocking collectives: none -> 398 us  [gather_turned(): shards = lax.all_to_all(shards, axis, split_axis=0, concat_axis=0)]
    all_gather x1 -> x0, waiting for transfers between devices: 53.7 us -> none  [gather_turned(): filled = lax.all_gather(both, axis, axis=0, tiled=True)]
    all_to_all x2 -> x1, blocking collectives: 36.8 us -> 18.4 us  [copy_for_each(): return lax.all_to_all(copies, axis, split_axis=0, concat_axis=0, tiled=True)]
    all_to_all x0 -> x1, waiting for transfers between devices: none -> 14.9 us  [copy_for_each(): return lax.all_to_all(copies, axis, split_axis=0, concat_axis=0, tiled=True)]
    all_to_all x1, blocking collectives: 27.3 us -> 21.4 us  [sum_at_owner(): lax.all_to_all(parts, axis, split_axis=0, concat_axis=0, tiled=True)]
  transfers between devices with their start and end apart: 2 -> 2, of which waited for: 2 -> 2; matrix products, arithmetic and copies ran while one was open for 5% -> 0% of each run, Pallas kernels for 0% -> 0%
where the time goes in v1:
time: 564 us; the launch traced here: 563 us
  blocking collectives  480 us (85%)
  waiting for transfers between devices  29.8 us (5%)
  matrix products  22.2 us (4%)
  starting transfers between devices  19.1 us (3%)
  local copies, waits for them, and re-layouts  6.52 us (1%)
    all_to_all x1, blocking collectives, gather_turned(): shards = lax.all_to_all(shards, axis, split_axis=0, concat_axis=0)  398 us
    all_gather x2, blocking collectives, gathered_once(): both, at, found = (lax.all_gather(jnp.concatenate(lines), axis), 0, {})  42 us
    all_to_all x1, blocking collectives, sum_at_owner(): lax.all_to_all(parts, axis, split_axis=0, concat_axis=0, tiled=True)  21.4 us
    all_to_all x1, blocking collectives, copy_for_each(): return lax.all_to_all(copies, axis, split_axis=0, concat_axis=0, tiled=True)  18.4 us
    all_to_all x1, waiting for transfers between devices, sum_at_owner(): lax.all_to_all(parts, axis, split_axis=0, concat_axis=0, tiled=True)  15 us
    all_to_all x1, waiting for transfers between devices, copy_for_each(): return lax.all_to_all(copies, axis, split_axis=0, concat_axis=0, tiled=True)  14.9 us
    all_to_all x1, starting transfers between devices, sum_at_owner(): lax.all_to_all(parts, axis, split_axis=0, concat_axis=0, tiled=True)  14.7 us
  transfers between devices with their start and end apart: 2, of which 2 were waited for; matrix products, arithmetic and copies ran while one was open for 0% of the time, Pallas kernels for 0%

profile of v1, /device:TPU:1, one launch (start us, length us, event | category | flops | bytes accessed | tf_op | source)
XLA Modules:
  0.0 562.5 jit_solution(12345478187086884484)
XLA Ops:
  0.0 0.9 convert.7
  0.9 1.1 divide_multiply_fusion
  2.0 12.2 %while.17 = (s32[]{:T(128)}, f32[1,128,128]{2,1,0:T(8,128)S(1)}, f32[1,128]{1,0:T(1,128)S(1)}, f32[4,1,64,128]{3,2,1,0:T(8,128)S(1)}, bf16[4,1,64,128]{3,2,1,0:T...) while((s32[]{:T(128)}, f32[1,128,128]{2,1,0:T(8,128)S(1)}, ...), condition=%wide.region_2.3_spmd.clone, body=%wide.region_0.2_spmd.clone.sunk | while | flops 8499459 | bytes 950424 | solution.py:167
  2.3 0.9 fusion.278
  3.3 0.9 fusion.282
  4.2 0.9 fusion.283
  5.4 0.9 fusion.278
  6.3 0.9 fusion.282
  7.3 0.9 fusion.283
  8.4 0.9 fusion.278
  9.4 0.9 fusion.282
  10.3 0.9 fusion.283
  11.5 0.9 fusion.278
  12.5 0.9 fusion.282
  13.4 0.9 fusion.283
  14.3 10.5 %all-gather.2 = bf16[4,129,128]{2,1,0:T(8,128)(2,1)S(1)} all-gather(bf16[1,129,128]{2,1,0:T(8,128)(2,1)S(1)} %maximum_bitcast_fusion), channel_id=2, replica_groups=mesh['sp_0'=16,'sp_1'=4,'tp'=8] {'sp_1'}, dimensions={0}, use_global_device_ids=true | all-gather | bytes 165120 | tf_op jit(solution)/shard_map/all_gather | solution.py:44
  24.9 31.6 %all-gather.3 = bf16[16,129,128]{2,1,0:T(8,128)(2,1)S(1)} all-gather(bf16[1,129,128]{2,1,0:T(8,128)(2,1)S(1)} %maximum_bitcast_fusion.1), channel_id=3, replica_groups=mesh['sp_0'=16,'sp_1'=4,'tp'=8] {'sp_0'}, dimensions={0}, use_global_device_ids=true | all-gather | bytes 561408 | tf_op jit(solution)/shard_map/all_gather | solution.py:44
  56.5 0.7 multiply_reduce_fusion
  57.5 1.4 convolution_convert_fusion
  58.9 14.7 %all-to-all-start = ((bf16[8,32,2048]{2,1,0:T(8,128)(2,1)}), bf16[8,32,2048]{2,1,0:T(8,128)(2,1)S(1)}, u32[]{:S(2)}, u32[]{:S(2)}) async-start(bf16[8,32,2048]{2,1,0:T(8,128)(2,1)} %bitcast.37), calls=%async_computation | async-start | bytes 2097152 | tf_op jit(solution)/shard_map/all_to_all | solution.py:83
  73.6 15.0 %all-to-all-done = bf16[8,32,2048]{2,1,0:T(8,128)(2,1)S(1)} async-done(((bf16[8,32,2048]{2,1,0:T(8,128)(2,1)}), bf16[8,32,2048]{2,1,0:T(8,128)(2,1)S(1)}, u32[]{:S(2)}, u32[]{:S(2)}) %all-to-all-start) | async-done | bytes 1048608 | tf_op jit(solution)/shard_map/all_to_all | solution.py:83
  88.7 1.1 fusion.65
  89.9 1.1 broadcast_in_dim.28
  91.0 4.4 all-to-all-start.1
  95.5 14.9 %all-to-all-done.1 = bf16[8,32,2048]{2,1,0:T(8,128)(2,1)S(1)} async-done(((bf16[8,32,2048]{2,1,0:T(8,128)(2,1)}), bf16[8,32,2048]{2,1,0:T(8,128)(2,1)S(1)}, u32[]{:S(2)}, u32[]{:S(2)}) %all-to-all-start.1) | async-done | bytes 1048608 | tf_op jit(solution)/shard_map/all_to_all | solution.py:89
  111.0 398.3 %all_to_all.25 = bf16[64,32,2112]{2,1,0:T(8,128)(2,1)S(1)} all-to-all(bf16[64,32,2112]{2,1,0:T(8,128)(2,1)S(1)} %stack.2), channel_id=1, replica_groups=mesh['sp_0'=16,'sp_1'=4,'tp'=8] {'sp_0','sp_1'}, dimensions={0} | all-to-all | bytes 17301504 | tf_op jit(solution)/shard_map/all_to_all | solution.py:19
  509.3 3.4 copy-done.1
  512.7 1.3 fusion.45
  514.1 7.3 %fusion.47 = bf16[256,2048]{1,0:T(8,128)(2,1)S(1)} fusion(bf16[2048,2112]{1,0:T(8,128)(2,1)} %bitcast.208, bf16[256,2048]{1,0:T(8,128)(2,1)S(1)} %bitcast.213, f32[256,704]{0,1:T(8,128)S(1)} %fusion.45), kind=kOutput, calls=%fused_computation.58 | convolution fusion | flops 1478000640 | bytes 9109504 | tf_op jit(solution)/shard_map/dot_general | solution.py:202
  521.4 21.4 %all_to_all.26 = bf16[8,32,2048]{2,1,0:T(8,128)(2,1)S(1)} all-to-all(bf16[8,32,2048]{2,1,0:T(8,128)(2,1)S(1)} %bitcast.214), channel_id=1, replica_groups=mesh['sp_0'=16,'sp_1'=4,'tp'=8] {'tp'}, dimensions={0} | all-to-all | bytes 2097152 | tf_op jit(solution)/shard_map/all_to_all | solution.py:83
  543.1 18.4 %all_to_all.27 = bf16[8,32,2048]{2,1,0:T(8,128)(2,1)S(1)} all-to-all(bf16[8,32,2048]{2,1,0:T(8,128)(2,1)S(1)} %broadcast_in_dim.29), channel_id=1, replica_groups=mesh['sp_0'=16,'sp_1'=4,'tp'=8] {'tp'}, dimensions={0} | all-to-all | bytes 2097152 | tf_op jit(solution)/shard_map/all_to_all | solution.py:89
  561.5 1.0 copy.36
  (73 shorter events, 2.9 us)
Async XLA Ops:
  0.0 57.5 %copy-start = (bf16[128,2048]{1,0:T(8,128)(2,1)S(1)}, bf16[128,2048]{1,0:T(8,128)(2,1)}, u32[]{:S(2)}) copy-start(bf16[128,2048]{1,0:T(8,128)(2,1)} %param.23) | copy-start | bytes 1572868
  14.2 43.1 %copy-start.2 = (bf16[256,128]{1,0:T(8,128)(2,1)S(1)}, bf16[256,128]{1,0:T(8,128)(2,1)}, u32[]{:S(2)}) copy-start(bf16[256,128]{1,0:T(8,128)(2,1)} %param.19) | copy-start | bytes 196612
  14.2 43.1 %copy-start.7 = (f32[128]{0:T(128)S(1)}, f32[128]{0:T(128)}, u32[]{:S(2)}) copy-start(f32[128]{0:T(128)} %param.22) | copy-start | bytes 1540
  57.2 32.5 %copy-start.6 = (f32[2048]{0:T(1024)S(1)}, f32[2048]{0:T(1024)}, u32[]{:S(2)}) copy-start(f32[2048]{0:T(1024)} %param.24) | copy-start | bytes 24580
  58.9 29.7 %all-to-all-start = ((bf16[8,32,2048]{2,1,0:T(8,128)(2,1)}), bf16[8,32,2048]{2,1,0:T(8,128)(2,1)S(1)}, u32[]{:S(2)}, u32[]{:S(2)}) async-start(bf16[8,32,2048]{2,1,0:T(8,128)(2,1)} %bitcast.37), calls=%async_computation | async-start | bytes 2097152 | tf_op jit(solution)/shard_map/all_to_all | solution.py:83
  73.6 21.8 %copy-start.3 = (bf16[32,704]{1,0:T(8,128)(2,1)S(1)}, bf16[32,704]{1,0:T(8,128)(2,1)}, u32[]{:S(2)}) copy-start(bf16[32,704]{1,0:T(8,128)(2,1)} %param.25) | copy-start | bytes 135172
  73.6 21.8 %copy-start.4 = (bf16[32,704]{1,0:T(8,128)(2,1)S(1)}, bf16[32,704]{1,0:T(8,128)(2,1)}, u32[]{:S(2)}) copy-start(bf16[32,704]{1,0:T(8,128)(2,1)} %param.26) | copy-start | bytes 135172
  73.6 21.8 %copy-start.5 = (bf16[704,32]{0,1:T(8,128)(2,1)S(1)}, bf16[704,32]{0,1:T(8,128)(2,1)}, u32[]{:S(2)}) copy-start(bf16[704,32]{0,1:T(8,128)(2,1)} %param.27) | copy-start | bytes 135172
  91.0 19.4 %all-to-all-start.1 = ((bf16[8,32,2048]{2,1,0:T(8,128)(2,1)}), bf16[8,32,2048]{2,1,0:T(8,128)(2,1)S(1)}, u32[]{:S(2)}, u32[]{:S(2)}) async-start(bf16[8,32,2048]{2,1,0:T(8,128)(2,1)} %broadcast_in_dim.28), calls=%async_computation.1 | async-start | bytes 2097152 | tf_op jit(solution)/shard_map/all_to_all | solution.py:89
  509.3 3.4 copy-start.1
